TPU v7x, 128 devices: a whole 4x4x4 slice. The times are simulated.
128 devices in a mesh: rep: 2 (over z_hi), fs: 32 (over z_lo, y, x), tp: 2 (over core).
Axes of the slice: x: 4, y: 4, z: 4 (z_hi: 2, z_lo: 2; z = z_hi * 2 + z_lo), core: 2. Of those that a mesh axis runs over, the one named last changes fastest.
Arguments:
- tokens: bfloat16 [49152, 2048], P(('rep', 'fs', 'tp')), may hold values from -6 to 6
- outer_weight: float32 [2048, 1536], P('fs', 'tp'), may hold values from -0.125 to 0.125
- inner_weight: float32 [2048, 1536], P('fs', 'tp'), may hold values from -0.125 to 0.125
- value_weight: float32 [2048, 1536], P('fs', 'tp'), may hold values from -0.125 to 0.125
- conv_taps: float32 [3, 1536], P(None, 'tp'), may hold values from -3 to 3
- mix_out: float32 [1536, 2048], P('tp', 'fs'), may hold values from -0.15625 to 0.15625
- norm_first: float32 [2048], replicated, may hold values from 0.1 to 1.9
- up_weight: float32 [2048, 4096], P('fs', 'tp'), may hold values from -0.125 to 0.125
- down_weight: float32 [4096, 2048], P('tp', 'fs'), may hold values from -0.09375 to 0.09375
- norm_second: float32 [2048], replicated, may hold values from 0.1 to 1.9
Outputs:
- encoded: bfloat16 [49152, 2048], P(('rep', 'fs', 'tp'))
All inputs are finite; a program needn't handle non-finite values.
Results may differ from a plain program's by a relative error of at most 0.015.
Values may be sent and summed in bfloat16 or wider, within the bound.
No kernel may reach another device: no remote copies, remote signals or barrier semaphores. Data moves between devices by JAX's collectives and lax.ppermute only.
A program may use at most 128 MiB of HBM per device.

v0:
```python
import jax
import jax.numpy as jnp
from jax import lax
from jax.sharding import Mesh
from jax.sharding import PartitionSpec as P

SEQ = 128
FS = ("fs_0", "fs_1", "fs_2")
REP_FS_TP = ("rep", "fs_0", "fs_1", "fs_2", "tp")


residual_scale = 2.0**0.25
norm_epsilon = 1e-05


def in_one_piece(arrays, axis, dim, along):
    ends, at = ([], 0)
    for a in arrays[:-1]:
        at += a.shape[along]
        ends.append(at)
    both = jnp.concatenate(arrays, axis=along)
    return tuple(jnp.split(lax.all_gather(both, axis, axis=dim, tiled=True), ends, axis=along))


def laid_out(tiles, dim):
    tiles = jnp.moveaxis(tiles, 0, dim)
    lengths = tiles.shape
    return tiles.reshape(*lengths[:dim], lengths[dim] * lengths[dim + 1], *lengths[dim + 2 :])


def stacked_from(x, axes, order):
    tiles = x
    for k in order:
        tiles = lax.all_gather(tiles, axes[k])
    done = order[::-1]
    back = [done.index(k) for k in range(len(axes))]
    tiles = tiles.transpose(*back, *range(len(axes), tiles.ndim))
    return tiles.reshape(-1, *x.shape)


def whole_of(x, axes, order, dim):
    return laid_out(stacked_from(x, axes, order), dim)


def cut_along(x, dim, length):
    before, after = (x.shape[:dim], x.shape[dim + 1 :])
    return jnp.moveaxis(x.reshape(*before, length, -1, *after), dim, 0)


def sum_at_owner(x, axis, dim):
    tiles = cut_along(x, dim, lax.axis_size(axis))
    arrived = lax.all_to_all(tiles, axis, split_axis=0, concat_axis=0, tiled=True)
    return arrived.astype(jnp.float32).sum(axis=0)


def layer_norm(values, scaling):
    center = values - jnp.mean(values, axis=-1, keepdims=True)
    spread = jnp.mean(center * center, axis=-1, keepdims=True)
    return center * lax.rsqrt(spread + norm_epsilon) * scaling


def short_conv(product, conv_taps):
    places = jnp.arange(product.shape[0], dtype=jnp.int32) % SEQ
    blank = jnp.zeros((1, product.shape[1]), jnp.float32)
    before = jnp.concatenate([blank, product[:-1]], axis=0)
    after = jnp.concatenate([product[1:], blank], axis=0)
    before = jnp.where((places > 0)[:, None], before, 0.0)
    after = jnp.where((places < SEQ - 1)[:, None], after, 0.0)
    return conv_taps[0] * before + conv_taps[1] * product + conv_taps[2] * after


def local(
    tokens,
    outer_weight,
    inner_weight,
    value_weight,
    conv_taps,
    mix_out,
    norm_first,
    up_weight,
    down_weight,
    norm_second,
):
    grouped = lax.all_gather(tokens, "tp", axis=0, tiled=True)
    outer_bf = outer_weight.astype(jnp.bfloat16)
    inner_bf = inner_weight.astype(jnp.bfloat16)
    value_bf = value_weight.astype(jnp.bfloat16)
    outer_full, inner_full, value_full = in_one_piece((outer_bf, inner_bf, value_bf), FS, 0, 1)
    outer = jnp.dot(grouped, outer_full, preferred_element_type=jnp.float32)
    inner = jnp.dot(grouped, inner_full, preferred_element_type=jnp.float32)
    value = jnp.dot(grouped, value_full, preferred_element_type=jnp.float32)
    mixed = (outer * short_conv(inner * value, conv_taps)).astype(jnp.bfloat16)
    mixout_full = whole_of(mix_out.astype(jnp.bfloat16), FS, (0, 1, 2), 1)
    selected = mixed
    mixing = sum_at_owner(
        jnp.dot(selected, mixout_full, preferred_element_type=jnp.float32).astype(jnp.bfloat16),
        "tp",
        0,
    )
    first = layer_norm(residual_scale * tokens.astype(jnp.float32) + mixing, norm_first).astype(
        jnp.bfloat16
    )
    grouped_first = lax.all_gather(first, "tp", axis=0, tiled=True)
    upward_bf = up_weight.astype(jnp.bfloat16)
    upward_full = lax.all_gather(upward_bf, FS, axis=0, tiled=True)
    raised = jnp.dot(grouped_first, upward_full, preferred_element_type=jnp.float32)
    raised = jax.nn.relu(raised)
    hidden = (raised * raised).astype(jnp.bfloat16)
    down_full = lax.all_gather(down_weight.astype(jnp.bfloat16), FS, axis=1, tiled=True)
    selected = hidden
    lowered = sum_at_owner(
        jnp.dot(selected, down_full, preferred_element_type=jnp.float32).astype(jnp.bfloat16),
        "tp",
        0,
    )
    return layer_norm(residual_scale * first.astype(jnp.float32) + lowered, norm_second).astype(
        jnp.bfloat16
    )


def solution(mesh):
    finer = Mesh(
        mesh.devices.reshape(mesh.shape["rep"], 2, 4, 4, mesh.shape["tp"]),
        ("rep", "fs_0", "fs_1", "fs_2", "tp"),
    )
    placed = (
        P(REP_FS_TP, None),
        P(FS, "tp"),
        P(FS, "tp"),
        P(FS, "tp"),
        P(None, "tp"),
        P("tp", FS),
        P(),
        P(FS, "tp"),
        P("tp", FS),
        P(),
    )
    return jax.shard_map(
        local, mesh=finer, in_specs=placed, out_specs=P(REP_FS_TP, None), check_vma=False
    )
```

profile of v0, /device:TPU:1, one launch (start us, length us, event | category | flops | bytes accessed | tf_op | source)
XLA Modules:
  0.0 637.7 jit_solution(7984287710747323062)
XLA Ops:
  6.6 1.0 convert_element_type.53
  7.6 5.6 all-gather
  13.3 13.2 %all-gather.1 = bf16[8,768,64]{1,2,0:T(8,128)(2,1)} all-gather(bf16[2,768,64]{1,2,0:T(8,128)(2,1)S(1)} %bitcast.37), channel_id=3, replica_groups=mesh['rep'=2,'fs_0'=2,'fs_1'=4,'fs_2'=4,'tp'=2] {'fs_1'}, dimensions={0}, use_global_device_ids=true | all-gather | bytes 983040 | tf_op jit(solution)/shard_map/all_gather | solution.py:34
  27.4 0.7 pad_maximum_fusion
  28.2 0.7 convert_element_type.58
  29.1 41.1 %all-gather.20.cloned.1.call-done = bf16[16,2,768,64]{2,3,1,0:T(8,128)(2,1)} async-done(((bf16[4,2,768,64]{2,3,1,0:T(8,128)(2,1)}), bf16[16,2,768,64]{2,3,1,0:T(8,128)(2,1)}) %all-gather.20.cloned.1.call-update) | async-done | bytes 3145744 | tf_op jit(solution)/shard_map/all_gather | solution.py:34
  70.2 3.9 copy.15
  74.1 13.4 %all-gather.12.cloned.1.call-done = bf16[768,2048]{1,0:T(8,128)(2,1)} async-done(((bf16[384,2048]{1,0:T(8,128)(2,1)}), bf16[768,2048]{1,0:T(8,128)(2,1)}) %all-gather.12.cloned.1.call-update) | async-done | bytes 3145744 | tf_op jit(solution)/shard_map/all_gather | solution.py:84
  87.5 149.6 %all-gather.10.cloned.1.call-done = bf16[2048,2304]{1,0:T(8,128)(2,1)} async-done(((bf16[64,2304]{1,0:T(8,128)(2,1)}), bf16[2048,2304]{1,0:T(8,128)(2,1)}) %all-gather.10.cloned.1.call-update) | async-done | bytes 9437200 | tf_op jit(solution)/shard_map/all_gather | solution.py:22
  237.1 5.6 fusion
  242.8 4.6 multiply_bitcast_fusion
  247.3 2.9 fusion.21
  250.3 13.9 %convolution_convert_fusion.1 = bf16[768,2048]{1,0:T(8,128)(2,1)} fusion(bf16[768,2048]{0,1:T(8,128)(2,1)} %bitcast.32, f32[767,768]{0,1:T(8,128)} %get-tuple-element.9, f32[768,768]{0,1:T(8,128)S(1)} %multiply_bitcast_fusion, f32[767,768]{0,1:T(8,128)} %get-tuple-element.8, bf16[768,2048]{1,0:T(8,128)(2,1)} %all-gather.12.cloned.1.call-done, ...), kind=kOutput, calls=%fused_computation.4 | convolution fusion | flops 4838719488 | bytes 19671552 | tf_op jit(solution)/shard_map/dot_general | solution.py:96
  264.2 28.7 %all_to_all.10 = bf16[2,384,2048]{2,1,0:T(8,128)(2,1)S(1)} all-to-all(bf16[2,384,2048]{2,1,0:T(8,128)(2,1)} %bitcast.33), channel_id=1, replica_groups=mesh['rep'=2,'fs_0'=2,'fs_1'=4,'fs_2'=4,'tp'=2] {'tp'}, dimensions={0} | all-to-all | bytes 6291456 | tf_op jit(solution)/shard_map/all_to_all | solution.py:52
  295.5 1.8 multiply_convert_fusion.2
  297.4 0.8 convert_element_type.60
  298.2 106.1 %all-gather.16.cloned.1.call-done = bf16[2048,2048]{1,0:T(8,128)(2,1)} async-done(((bf16[64,2048]{1,0:T(8,128)(2,1)}), bf16[2048,2048]{1,0:T(8,128)(2,1)}) %all-gather.16.cloned.1.call-update) | async-done | bytes 8388624 | tf_op jit(solution)/shard_map/all_gather | solution.py:105
  404.2 37.8 %all-gather.14.cloned.1.call-done = bf16[768,2048]{1,0:T(8,128)(2,1)} async-done(((bf16[384,2048]{1,0:T(8,128)(2,1)}), bf16[768,2048]{1,0:T(8,128)(2,1)}) %all-gather.14.cloned.1.call-update) | async-done | bytes 3145744 | tf_op jit(solution)/shard_map/all_gather | solution.py:103
  442.1 10.0 %multiply_convert_fusion = bf16[768,2048]{1,0:T(8,128)(2,1)S(1)} fusion(bf16[768,2048]{1,0:T(8,128)(2,1)} %all-gather.14.cloned.1.call-done, bf16[2048,2048]{1,0:T(8,128)(2,1)} %all-gather.16.cloned.1.call-done), kind=kOutput, calls=%fused_computation.1 | convolution fusion | flops 6447169536 | bytes 14680064 | tf_op jit(solution)/shard_map/dot_general | solution.py:106
  452.1 138.3 %all-gather.18.cloned.1.call-done = bf16[2048,2048]{0,1:T(8,128)(2,1)} async-done(((bf16[2048,64]{0,1:T(8,128)(2,1)}), bf16[2048,2048]{0,1:T(8,128)(2,1)}) %all-gather.18.cloned.1.call-update) | async-done | bytes 8388624 | tf_op jit(solution)/shard_map/all_gather | solution.py:109
  590.4 9.1 %convolution_convert_fusion = bf16[768,2048]{1,0:T(8,128)(2,1)S(1)} fusion(bf16[768,2048]{1,0:T(8,128)(2,1)S(1)} %multiply_convert_fusion, bf16[2048,2048]{0,1:T(8,128)(2,1)} %all-gather.18.cloned.1.call-done), kind=kOutput, calls=%fused_computation.3 | convolution fusion | flops 6444023808 | bytes 14680064 | tf_op jit(solution)/shard_map/dot_general | solution.py:112
  599.5 26.9 %all_to_all.11 = bf16[2,384,2048]{2,1,0:T(8,128)(2,1)S(1)} all-to-all(bf16[2,384,2048]{2,1,0:T(8,128)(2,1)S(1)} %bitcast.34), channel_id=1, replica_groups=mesh['rep'=2,'fs_0'=2,'fs_1'=4,'fs_2'=4,'tp'=2] {'tp'}, dimensions={0} | all-to-all | bytes 6291456 | tf_op jit(solution)/shard_map/all_to_all | solution.py:52
  626.4 0.7 convert_reduce_fusion
  629.1 1.8 multiply_convert_fusion.1
  (49 shorter events, 5.6 us)
Async XLA Ops:
  6.5 20.8 %copy-start.4 = (f32[64,768]{1,0:T(8,128)S(1)}, f32[64,768]{1,0:T(8,128)}, u32[]{:S(2)}) copy-start(f32[64,768]{1,0:T(8,128)} %param.11) | copy-start | bytes 589828
  6.5 20.8 %copy-start.5 = (f32[64,768]{1,0:T(8,128)S(1)}, f32[64,768]{1,0:T(8,128)}, u32[]{:S(2)}) copy-start(f32[64,768]{1,0:T(8,128)} %param.12) | copy-start | bytes 589828
  6.5 20.8 %copy-start.6 = (f32[64,768]{1,0:T(8,128)S(1)}, f32[64,768]{1,0:T(8,128)}, u32[]{:S(2)}) copy-start(f32[64,768]{1,0:T(8,128)} %param.13) | copy-start | bytes 589828
  6.5 21.7 %copy-start.2 = (f32[64,2048]{1,0:T(8,128)S(1)}, f32[64,2048]{1,0:T(8,128)}, u32[]{:S(2)}) copy-start(f32[64,2048]{1,0:T(8,128)} %param.17) | copy-start | bytes 1572868
  6.5 63.7 %all-gather.20.cloned.1.call-start = ((), (), s32[]{:S(2)}) async-start(), calls=%async_computation.7 | async-start | bytes 3932160 | tf_op jit(solution)/shard_map/all_gather | solution.py:34
  13.2 15.8 %copy-start.9 = (f32[3,768]{1,0:T(4,128)S(1)}, f32[3,768]{1,0:T(4,128)}, u32[]{:S(2)}) copy-start(f32[3,768]{1,0:T(4,128)} %param.14) | copy-start | bytes 27652
  26.5 61.0 %all-gather.12.cloned.1.call-start = ((), (), s32[]{:S(2)}) async-start(), calls=%async_computation.3 | async-start | bytes 4718592 | tf_op jit(solution)/shard_map/all_gather | solution.py:84
  27.3 209.8 %all-gather.10.cloned.1.call-start = ((), (), s32[]{:S(2)}) async-start(), calls=%async_computation.2 | async-start | bytes 9732096 | tf_op jit(solution)/shard_map/all_gather | solution.py:22
  28.2 376.1 %all-gather.16.cloned.1.call-start = ((), (), s32[]{:S(2)}) async-start(), calls=%async_computation.5 | async-start | bytes 8650752 | tf_op jit(solution)/shard_map/all_gather | solution.py:105
  29.0 413.1 %all-gather.14.cloned.1.call-start = ((), (), s32[]{:S(2)}) async-start(), calls=%async_computation.4 | async-start | bytes 4718592 | tf_op jit(solution)/shard_map/all_gather | solution.py:103
  237.1 5.7 copy-start.10
  292.8 1.4 copy-start.1
  294.7 0.7 copy-start.7
  295.5 1.9 copy-start.3
  297.3 293.0 %all-gather.18.cloned.1.call-start = ((), (), s32[]{:S(2)}) async-start(), calls=%async_computation.6 | async-start | bytes 8650752 | tf_op jit(solution)/shard_map/all_gather | solution.py:109
  626.4 1.4 copy-start
  628.3 0.7 copy-start.8
Sparse Core Ops, SparseCore 0:
  26.6 43.5 all-gather.19
  71.9 15.6 all-gather.11
  89.2 147.8 all-gather.9
  238.6 165.6 all-gather.15
  405.7 36.2 all-gather.13
  443.6 146.7 all-gather.17
where the time goes:
time: 638 us
  waiting for transfers between devices  487 us (76%)
  blocking collectives  74.4 us (12%)
  matrix products  43.3 us (7%)
  between operations  13.7 us (2%)
  other arithmetic  10.8 us (2%)
  local copies, waits for them, and re-layouts  8.27 us (1%)
    all_gather x1, waiting for transfers between devices, in_one_piece(): lax.all_gather(both, axis, axis=dim, tiled=True)  150 us
    all_gather x1, waiting for transfers between devices, local(): lax.all_gather(down_weight.astype(jnp.bfloat16), FS, axis=1, tiled=True)  138 us
    all_gather x1, waiting for transfers between devices, local(): upward_full = lax.all_gather(upward_bf, FS, axis=0, tiled=True)  106 us
    all_to_all x2, blocking collectives, sum_at_owner(): lax.all_to_all(tiles, axis, split_axis=0, concat_axis=0, tiled=True)  55.6 us
    all_gather x1, waiting for transfers between devices, stacked_from(): tiles = lax.all_gather(tiles, axes[k])  41.1 us
    all_gather x1, waiting for transfers between devices, local(): grouped_first = lax.all_gather(first, 'tp', axis=0, tiled=True)  37.8 us
    all_gather x2, blocking collectives, stacked_from(): tiles = lax.all_gather(tiles, axes[k])  18.8 us
    dot_general x1, matrix products, local(): jnp.dot(selected, mixout_full, preferred_element_type=jnp.float32)  13.9 us
  transfers between devices with their start and end apart: 6, of which 6 were waited for; matrix products, arithmetic and copies ran while one was open for 7% of the time, Pallas kernels for 0%

commit v1 on v0

v1 whole, which is shorter than its diff:
```python
import jax
import jax.numpy as jnp
from jax import lax
from jax.sharding import Mesh
from jax.sharding import PartitionSpec as P

SEQ = 128
FS = ("fs_0", "fs_1", "fs_2")
REP_FS = ("rep", "fs_0", "fs_1", "fs_2")
REP_FS_TP = ("rep", "fs_0", "fs_1", "fs_2", "tp")


residual_scale = 2.0**0.25
norm_epsilon = 1e-05


def own_half(x, dim):
    length = x.shape[dim] // 2
    return lax.dynamic_slice_in_dim(x, lax.axis_index("rep") * length, length, dim)


def gathered_halves(x):
    full = lax.all_gather(x, REP_FS, axis=0, tiled=True)
    return full.reshape(2, -1, x.shape[1])


def sum_at_owner(x, axis):
    tiles = x.reshape(2, -1, x.shape[1])
    arrived = lax.all_to_all(tiles, axis, split_axis=0, concat_axis=0, tiled=True)
    return arrived.astype(jnp.float32).sum(axis=0)


def layer_norm(values, scaling):
    center = values - jnp.mean(values, axis=-1, keepdims=True)
    spread = jnp.mean(center * center, axis=-1, keepdims=True)
    return center * lax.rsqrt(spread + norm_epsilon) * scaling


def short_conv(product, conv_taps):
    places = jnp.arange(product.shape[0], dtype=jnp.int32) % SEQ
    blank = jnp.zeros((1, product.shape[1]), jnp.float32)
    before = jnp.concatenate([blank, product[:-1]], axis=0)
    after = jnp.concatenate([product[1:], blank], axis=0)
    before = jnp.where((places > 0)[:, None], before, 0.0)
    after = jnp.where((places < SEQ - 1)[:, None], after, 0.0)
    return conv_taps[0] * before + conv_taps[1] * product + conv_taps[2] * after


def dot(a, b):
    return jnp.dot(a, b, preferred_element_type=jnp.float32)


def dot_t(a, b):
    return lax.dot_general(a, b, (((1,), (1,)), ((), ())), preferred_element_type=jnp.float32)


def local(
    tokens,
    outer_weight,
    inner_weight,
    value_weight,
    conv_taps,
    mix_out,
    norm_first,
    up_weight,
    down_weight,
    norm_second,
):
    bf = jnp.bfloat16
    grouped = lax.all_gather(tokens, "tp", axis=0, tiled=True)
    into = jnp.concatenate(
        [own_half(w, 1).astype(bf) for w in (outer_weight, inner_weight, value_weight)], axis=1
    )
    into_full = gathered_halves(into)
    mixout_full = gathered_halves(own_half(mix_out, 0).astype(bf).T)
    up_full = gathered_halves(own_half(up_weight, 1).astype(bf))
    down_full = gathered_halves(own_half(down_weight, 0).astype(bf).T)

    width = into.shape[1] // 3
    mixing = 0.0
    for h in range(2):
        w = into_full[h]
        outer = dot(grouped, w[:, :width])
        inner = dot(grouped, w[:, width : 2 * width])
        value = dot(grouped, w[:, 2 * width :])
        taps = conv_taps[:, h * width : (h + 1) * width]
        mixed = (outer * short_conv(inner * value, taps)).astype(bf)
        mixing = mixing + dot_t(mixed, mixout_full[h])
    mixing = sum_at_owner(mixing.astype(bf), "tp")
    first = layer_norm(residual_scale * tokens.astype(jnp.float32) + mixing, norm_first).astype(bf)
    grouped_first = lax.all_gather(first, "tp", axis=0, tiled=True)
    lowered = 0.0
    for h in range(2):
        raised = jax.nn.relu(dot(grouped_first, up_full[h]))
        hidden = (raised * raised).astype(bf)
        lowered = lowered + dot_t(hidden, down_full[h])
    lowered = sum_at_owner(lowered.astype(bf), "tp")
    return layer_norm(residual_scale * first.astype(jnp.float32) + lowered, norm_second).astype(bf)


def solution(mesh):
    finer = Mesh(
        mesh.devices.reshape(mesh.shape["rep"], 2, 4, 4, mesh.shape["tp"]),
        ("rep", "fs_0", "fs_1", "fs_2", "tp"),
    )
    placed = (
        P(REP_FS_TP, None),
        P(FS, "tp"),
        P(FS, "tp"),
        P(FS, "tp"),
        P(None, "tp"),
        P("tp", FS),
        P(),
        P(FS, "tp"),
        P("tp", FS),
        P(),
    )
    return jax.shard_map(
        local, mesh=finer, in_specs=placed, out_specs=P(REP_FS_TP, None), check_vma=False
    )
```

time: 638 us -> 386 us (0.61)
  waiting for transfers between devices: 487 us -> 282 us
  blocking collectives: 74.4 us -> 16.1 us
  matrix products: 43.3 us -> 54.6 us
    all_gather x4, waiting for transfers between devices: 435 us -> 250 us  [gathered_halves(): full = lax.all_gather(x, REP_FS, axis=0, tiled=True)]
    all_to_all x2, blocking collectives: 55.6 us -> 16.1 us  [sum_at_owner(): lax.all_to_all(tiles, axis, split_axis=0, concat_axis=0, tiled=True)]
    all_gather x1, waiting for transfers between devices: 37.8 us -> 16.5 us  [local(): grouped_first = lax.all_gather(first, 'tp', axis=0, tiled=True)]
    all_gather x2 -> x0, blocking collectives: 18.8 us -> none  [stacked_from(): tiles = lax.all_gather(tiles, axes[k])]
    dot_general x5 -> x10, matrix products: 43.3 us -> 54.6 us  [the longest x4 30.7 us: dot_t(): lax.dot_general(a, b, (((1,), (1,)), ((), ())), preferred_element_type=jn...]
  transfers between devices with their start and end apart: 6 -> 6, of which waited for: 6 -> 6; matrix products, arithmetic and copies ran while one was open for 7% -> 16% of each run, Pallas kernels for 0% -> 0%
where the time goes in v1:
time: 386 us
  waiting for transfers between devices  282 us (73%)
  matrix products  54.6 us (14%)
  blocking collectives  16.1 us (4%)
  between operations  13.7 us (4%)
  local copies, waits for them, and re-layouts  11.4 us (3%)
  other arithmetic  8.22 us (2%)
    all_gather x4, waiting for transfers between devices, gathered_halves(): full = lax.all_gather(x, REP_FS, axis=0, tiled=True)  250 us
    dot_general x4, matrix products, dot_t(): lax.dot_general(a, b, (((1,), (1,)), ((), ())), preferred_element_type=jn...  30.7 us
    dot_general x6, matrix products, dot(): return jnp.dot(a, b, preferred_element_type=jnp.float32)  24 us
    all_gather x1, waiting for transfers between devices, local(): grouped_first = lax.all_gather(first, 'tp', axis=0, tiled=True)  16.5 us
    all_to_all x2, blocking collectives, sum_at_owner(): lax.all_to_all(tiles, axis, split_axis=0, concat_axis=0, tiled=True)  16.1 us
    all_gather x1, waiting for transfers between devices, local(): grouped = lax.all_gather(tokens, 'tp', axis=0, tiled=True)  14.3 us
  transfers between devices with their start and end apart: 6, of which 6 were waited for; matrix products, arithmetic and copies ran while one was open for 16% of the time, Pallas kernels for 0%

profile of v1, /device:TPU:1, one launch (start us, length us, event | category | flops | bytes accessed | tf_op | source)
XLA Modules:
  0.0 385.9 jit_solution(15496005332504647773)
XLA Ops:
  9.9 1.5 fusion.87
  13.1 14.3 %all-gather.9.cloned.1.call-done = bf16[768,2048]{1,0:T(8,128)(2,1)} async-done(((bf16[384,2048]{1,0:T(8,128)(2,1)}), bf16[768,2048]{1,0:T(8,128)(2,1)}) %all-gather.9.cloned.1.call-update) | async-done | bytes 3145744 | tf_op jit(solution)/shard_map/all_gather | solution.py:70
  27.5 84.8 %all-gather.7.cloned.1.call-done = bf16[4096,1152]{1,0:T(8,128)(2,1)} async-done(((bf16[64,1152]{1,0:T(8,128)(2,1)}), bf16[4096,1152]{1,0:T(8,128)(2,1)}) %all-gather.7.cloned.1.call-update) | async-done | bytes 9437200 | tf_op jit(solution)/shard_map/all_gather | solution.py:23
  112.3 4.0 %fusion.23 = f32[384,768]{1,0:T(8,128)S(1)} fusion(bf16[768,2048]{1,0:T(8,128)(2,1)} %all-gather.9.cloned.1.call-done, bf16[4096,1152]{1,0:T(8,128)(2,1)} %all-gather.7.cloned.1.call-done), kind=kOutput, calls=%fused_computation.29 | convolution fusion | flops 1207959552 | bytes 5898240 | tf_op jit(solution)/shard_map/dot_general | solution.py:50
  116.3 2.9 fusion.50
  119.2 1.8 fusion.96
  121.0 2.9 fusion.15
  123.9 2.9 fusion.47
  126.8 1.8 fusion.95
  128.6 51.8 %all-gather.11.cloned.1.call-done = bf16[4096,384]{1,0:T(8,128)(2,1)} async-done(((bf16[64,384]{1,0:T(8,128)(2,1)}), bf16[4096,384]{1,0:T(8,128)(2,1)}) %all-gather.11.cloned.1.call-update) | async-done | bytes 3145744 | tf_op jit(solution)/shard_map/all_gather | solution.py:23
  180.3 10.2 %fusion.21 = f32[768,2048]{1,0:T(8,128)} fusion(bf16[4096,384]{1,0:T(8,128)(2,1)} %all-gather.11.cloned.1.call-done, bf16[768,2048]{1,0:T(8,128)(2,1)} %all-gather.9.cloned.1.call-done, bf16[4096,1152]{1,0:T(8,128)(2,1)} %all-gather.7.cloned.1.call-done, f32[767,384]{0,1:T(8,128)} %get-tuple-element.14, f32[768,384]{0,1:T(8,128)S(1)} %fusion.50, ...), kind=kOutput, calls=%fused_computation.27 | convolution fusion | flops 2418573312 | bytes 16128000 | tf_op jit(solution)/shard_map/dot_general | solution.py:54
  190.6 11.4 %add_convert_fusion.1 = bf16[768,2048]{1,0:T(8,128)(2,1)} fusion(f32[768,2048]{1,0:T(8,128)} %fusion.21, bf16[4096,384]{1,0:T(8,128)(2,1)} %all-gather.11.cloned.1.call-done, bf16[768,2048]{1,0:T(8,128)(2,1)} %all-gather.9.cloned.1.call-done, bf16[4096,1152]{1,0:T(8,128)(2,1)} %all-gather.7.cloned.1.call-done, f32[767,384]{0,1:T(8,128)} %get-tuple-element.12, ...), kind=kOutput, calls=%fused_computation.3 | convolution fusion | flops 2421719040 | bytes 19273728 | tf_op jit(solution)/shard_map/dot_general | solution.py:54
  201.9 9.3 %all_to_all.10 = bf16[2,384,2048]{2,1,0:T(8,128)(2,1)S(1)} all-to-all(bf16[2,384,2048]{2,1,0:T(8,128)(2,1)} %bitcast.36), channel_id=1, replica_groups=mesh['rep'=2,'fs_0'=2,'fs_1'=4,'fs_2'=4,'tp'=2] {'tp'}, dimensions={0} | all-to-all | bytes 6291456 | tf_op jit(solution)/shard_map/all_to_all | solution.py:29
  213.8 1.8 multiply_convert_fusion.3
  215.8 1.6 fusion.86
  217.4 42.8 %all-gather.15.cloned.1.call-done = bf16[4096,1024]{1,0:T(8,128)(2,1)} async-done(((bf16[64,1024]{1,0:T(8,128)(2,1)}), bf16[4096,1024]{1,0:T(8,128)(2,1)}) %all-gather.15.cloned.1.call-update) | async-done | bytes 8388624 | tf_op jit(solution)/shard_map/all_gather | solution.py:23
  260.2 16.5 %all-gather.13.cloned.1.call-done = bf16[768,2048]{1,0:T(8,128)(2,1)} async-done(((bf16[384,2048]{1,0:T(8,128)(2,1)}), bf16[768,2048]{1,0:T(8,128)(2,1)}) %all-gather.13.cloned.1.call-update) | async-done | bytes 3145744 | tf_op jit(solution)/shard_map/all_gather | solution.py:91
  276.7 6.7 %multiply_convert_fusion.1 = bf16[768,1024]{1,0:T(8,128)(2,1)S(1)} fusion(bf16[768,2048]{1,0:T(8,128)(2,1)} %all-gather.13.cloned.1.call-done, bf16[4096,1024]{1,0:T(8,128)(2,1)} %all-gather.15.cloned.1.call-done), kind=kOutput, calls=%fused_computation.14 | convolution fusion | flops 3223584768 | bytes 8912896 | tf_op jit(solution)/shard_map/dot_general | solution.py:50
  283.4 4.6 %multiply_convert_fusion.2 = bf16[768,1024]{1,0:T(8,128)(2,1)} fusion(bf16[768,2048]{1,0:T(8,128)(2,1)S(1)} %copy-done.9, bf16[4096,1024]{1,0:T(8,128)(2,1)S(1)} %copy-done.7), kind=kOutput, calls=%fused_computation.15 | convolution fusion | flops 3223584768 | bytes 8912896 | tf_op jit(solution)/shard_map/dot_general | solution.py:50
  288.0 70.6 %all-gather.17.cloned.1.call-done = bf16[4096,1024]{1,0:T(8,128)(2,1)} async-done(((bf16[64,1024]{1,0:T(8,128)(2,1)}), bf16[4096,1024]{1,0:T(8,128)(2,1)}) %all-gather.17.cloned.1.call-update) | async-done | bytes 8388624 | tf_op jit(solution)/shard_map/all_gather | solution.py:23
  358.6 5.4 %fusion = f32[768,2048]{1,0:T(8,128)S(1)} fusion(bf16[768,1024]{1,0:T(8,128)(2,1)S(1)} %multiply_convert_fusion.1, bf16[4096,1024]{1,0:T(8,128)(2,1)} %all-gather.17.cloned.1.call-done), kind=kOutput, calls=%fused_computation.4 | convolution fusion | flops 3221225472 | bytes 12058624 | tf_op jit(solution)/shard_map/dot_general | solution.py:54
  364.1 3.7 add_convert_fusion
  367.8 6.8 %all_to_all.11 = bf16[2,384,2048]{2,1,0:T(8,128)(2,1)S(1)} all-to-all(bf16[2,384,2048]{2,1,0:T(8,128)(2,1)S(1)} %bitcast.37), channel_id=1, replica_groups=mesh['rep'=2,'fs_0'=2,'fs_1'=4,'fs_2'=4,'tp'=2] {'tp'}, dimensions={0} | all-to-all | bytes 6291456 | tf_op jit(solution)/shard_map/all_to_all | solution.py:29
  377.2 1.8 multiply_convert_fusion
  (50 shorter events, 10.3 us)
Async XLA Ops:
  6.5 5.0 %copy-start = (f32[64,2048]{1,0:T(8,128)S(1)}, f32[64,2048]{1,0:T(8,128)}, u32[]{:S(2)}) copy-start(f32[64,2048]{1,0:T(8,128)} %param.17) | copy-start | bytes 1572868
  6.5 20.9 %all-gather.9.cloned.1.call-start = ((), (), s32[]{:S(2)}) async-start(), calls=%async_computation.3 | async-start | bytes 4718592 | tf_op jit(solution)/shard_map/all_gather | solution.py:70
  7.3 105.0 %all-gather.7.cloned.1.call-start = ((), (), s32[]{:S(2)}) async-start(), calls=%async_computation.2 | async-start | bytes 9584640 | tf_op jit(solution)/shard_map/all_gather | solution.py:23
  9.9 170.5 %all-gather.11.cloned.1.call-start = ((), (), s32[]{:S(2)}) async-start(), calls=%async_computation.4 | async-start | bytes 3194880 | tf_op jit(solution)/shard_map/all_gather | solution.py:23
  11.5 248.7 %all-gather.15.cloned.1.call-start = ((), (), s32[]{:S(2)}) async-start(), calls=%async_computation.6 | async-start | bytes 8519680 | tf_op jit(solution)/shard_map/all_gather | solution.py:23
  12.2 264.5 %all-gather.13.cloned.1.call-start = ((), (), s32[]{:S(2)}) async-start(), calls=%async_computation.5 | async-start | bytes 4718592 | tf_op jit(solution)/shard_map/all_gather | solution.py:91
  112.3 4.0 %copy-start.4 = (bf16[768,2048]{1,0:T(8,128)(2,1)S(1)}, bf16[768,2048]{1,0:T(8,128)(2,1)}, u32[]{:S(2)}) copy-start(bf16[768,2048]{1,0:T(8,128)(2,1)} %all-gather.9.cloned.1.call-done) | copy-start | bytes 9437188
  211.2 1.4 copy-start.3
  213.1 0.7 copy-start.5
  215.7 142.9 %all-gather.17.cloned.1.call-start = ((), (), s32[]{:S(2)}) async-start(), calls=%async_computation.7 | async-start | bytes 8519680 | tf_op jit(solution)/shard_map/all_gather | solution.py:23
  276.7 6.7 %copy-start.7 = (bf16[4096,1024]{1,0:T(8,128)(2,1)S(1)}, bf16[4096,1024]{1,0:T(8,128)(2,1)}, u32[]{:S(2)}) copy-start(bf16[4096,1024]{1,0:T(8,128)(2,1)} %all-gather.15.cloned.1.call-done) | copy-start | bytes 25165828
  276.7 6.7 %copy-start.9 = (bf16[768,2048]{1,0:T(8,128)(2,1)S(1)}, bf16[768,2048]{1,0:T(8,128)(2,1)}, u32[]{:S(2)}) copy-start(bf16[768,2048]{1,0:T(8,128)(2,1)} %all-gather.13.cloned.1.call-done) | copy-start | bytes 9437188
  358.6 5.4 %copy-start.8 = (bf16[4096,1024]{1,0:T(8,128)(2,1)S(1)}, bf16[4096,1024]{1,0:T(8,128)(2,1)}, u32[]{:S(2)}) copy-start(bf16[4096,1024]{1,0:T(8,128)(2,1)} %all-gather.17.cloned.1.call-done) | copy-start | bytes 25165828
  358.6 5.4 %copy-start.10 = (bf16[768,1024]{1,0:T(8,128)(2,1)S(1)}, bf16[768,1024]{1,0:T(8,128)(2,1)}, u32[]{:S(2)}) copy-start(bf16[768,1024]{1,0:T(8,128)(2,1)} %multiply_convert_fusion.2) | copy-start | bytes 4718596
  374.6 1.4 copy-start.2
  376.5 0.7 copy-start.6
  377.2 1.9 copy-start.1
Sparse Core Ops, SparseCore 0:
  9.0 18.4 all-gather.8
  30.2 82.0 all-gather.6
  115.1 65.2 all-gather.10
  183.1 77.0 all-gather.14
  261.7 14.9 all-gather.12
  279.4 79.1 all-gather.16
